TPU v7x, 256 devices: a whole 4x4x8 slice. The times are simulated.
256 devices in a mesh: kv: 32 (over z, y), tp: 8 (over x, core).
Axes of the slice: x: 4, y: 4, z: 8, core: 2. Of those that a mesh axis runs over, the one named last changes fastest.
Arguments:
- tokens: bfloat16 [32, 4096], P(None, ('kv', 'tp')), may hold values from -24 to 24
- attention_norm_gain: float32 [4096], P('kv'), may hold values from 0.1 to 1.9
- query_first: bfloat16 [4096, 2048], P('kv', 'tp'), may hold values from -0.09375 to 0.09375
- query_second: bfloat16 [4096, 2048], P('kv', 'tp'), may hold values from -0.09375 to 0.09375
- key_first: bfloat16 [4096, 512], P('kv', 'tp'), may hold values from -0.15625 to 0.15625
- key_second: bfloat16 [4096, 512], P('kv', 'tp'), may hold values from -0.15625 to 0.15625
- value_weight: bfloat16 [4096, 1024], P('kv', 'tp'), may hold values from -0.09375 to 0.09375
- key_cache: bfloat16 [32, 16384, 8, 128], P(None, 'kv', 'tp'), may hold values from -270 to 270
- value_cache: bfloat16 [32, 16384, 8, 128], P(None, 'kv', 'tp'), may hold values from -6 to 6
- lambdas: float32 [32], P('tp'), may hold values from 0.3 to 0.8
- head_gain: float32 [128], replicated, may hold values from 0.1 to 1.9
- out_weight: bfloat16 [4096, 4096], P('tp', 'kv'), may hold values from -0.09375 to 0.09375
- mlp_gain: float32 [4096], P('kv'), may hold values from 0.1 to 1.9
- gate_weight: bfloat16 [4096, 11264], P('kv', 'tp'), may hold values from -0.09375 to 0.09375
- up_weight: bfloat16 [4096, 11264], P('kv', 'tp'), may hold values from -0.09375 to 0.09375
- down_projection_weight: bfloat16 [11264, 4096], P('tp', 'kv'), may hold values from -0.109375 to 0.109375
Outputs:
- layer_out: bfloat16 [32, 4096], P(None, ('kv', 'tp'))
- incoming_key_pair: bfloat16 [32, 8, 128], P(None, 'tp')
- new_values: bfloat16 [32, 8, 128], P(None, 'tp')
All inputs are finite; a program needn't handle non-finite values.
Results may differ from a plain program's by a relative error of at most 0.014.
Values may be sent and summed in bfloat16 or wider, within the bound.
A program may use at most 64 MiB of HBM per device.

v0:
```python
import math

import jax
import jax.numpy as jnp
from jax import lax
from jax.sharding import PartitionSpec as P

D = 4096
HEAD_DIM = 64


EPS = 1e-06


def sent_to_all(x, axis):
    copies = jnp.broadcast_to(x, (lax.axis_size(axis), *x.shape))
    return lax.all_to_all(copies, axis, split_axis=0, concat_axis=0, tiled=True)


def joined_along(tiles, dim):
    lengths = list(tiles.shape[1:])
    lengths[dim] *= tiles.shape[0]
    return jnp.moveaxis(tiles, 0, dim).reshape(lengths)


def collect(x, axis, dim):
    tiles = sent_to_all(x, axis)
    return joined_along(tiles, dim)


def padded_to(lines, length):
    spare = -lines.shape[0] % length
    if not spare:
        return lines
    return jnp.concatenate([lines, jnp.zeros((spare, *lines.shape[1:]), lines.dtype)])


def in_blocks(x, dim, length):
    before, after = (x.shape[:dim], x.shape[dim + 1 :])
    return jnp.moveaxis(x.reshape(*before, length, -1, *after), dim, 0)


def sum_at_owner(x, axis, dim):
    length = lax.axis_size(axis)
    tiles = lax.all_to_all(in_blocks(x, dim, length), axis, 0, 0, tiled=True)
    return jnp.sum(tiles, axis=0)


def nested_sum(x, axes):
    padded = padded_to(x, lax.axis_size(axes))
    whole = collect(sum_at_owner(padded, axes, 0), axes, 0)
    return lax.slice_in_dim(whole, 0, len(x)).reshape(x.shape)


def packed_total(arrays, axis):
    ravelled, at, gathered = (jnp.concatenate([a.reshape(-1) for a in arrays]), 0, [])
    subtotal = nested_sum(ravelled, axis)
    for a in arrays:
        gathered.append(subtotal[at : at + a.size].reshape(a.shape))
        at += a.size
    return tuple(gathered)


def side_by_side(arrays, axis, split_dim, concat_dim, along):
    widths = [math.prod(a.shape[along:]) for a in arrays]
    both = jnp.concatenate(
        [a.reshape(*a.shape[:along], w) for a, w in zip(arrays, widths)], axis=along
    )
    out = lax.all_to_all(both, axis, split_axis=split_dim, concat_axis=concat_dim, tiled=True)
    tiles = jnp.split(out, [sum(widths[:k]) for k in range(1, len(widths))], axis=along)
    return tuple((b.reshape(*out.shape[:along], *a.shape[along:]) for a, b in zip(arrays, tiles)))


def summed_on_arrival(x, axis, dim):
    length = lax.axis_size(axis)
    tiles = lax.all_to_all(in_blocks(x, dim, length), axis, 0, 0, tiled=True)
    return jnp.sum(tiles.astype(jnp.float32), axis=0)


def source_positions(pieces):
    result = []
    for offset in (0, 3):
        tops, totals, weighted = (pieces[offset], pieces[offset + 1], pieces[offset + 2])
        top = jnp.max(tops, axis=0)
        scales = jnp.exp(tops - top[None])
        result.extend(
            [top, jnp.sum(totals * scales, axis=0), jnp.sum(weighted * scales[:, :, None], axis=0)]
        )
    return tuple(result)


def finish(merged, lam_rows, head_gain):
    first = merged[2] / merged[1][:, None]
    second = merged[5] / merged[4][:, None]
    mixed = first - lam_rows[:, None] * second
    normed = mixed * lax.rsqrt(jnp.mean(mixed * mixed, axis=1, keepdims=True) + EPS) * head_gain
    return normed.astype(jnp.bfloat16)


def shards(
    tokens,
    attention_norm_gain,
    query_first,
    query_second,
    key_first,
    key_second,
    value_weight,
    key_cache,
    value_cache,
    lambdas,
    head_gain,
    out_weight,
    mlp_gain,
    gate_weight,
    up_weight,
    down_projection_weight,
):
    batch = tokens.shape[0]
    head_local = query_first.shape[1] // HEAD_DIM
    kv_local = key_first.shape[1] // HEAD_DIM
    group = head_local // kv_local
    scale = HEAD_DIM ** (-0.5)
    rows_block = collect(tokens, "tp", 1)
    wide = rows_block.astype(jnp.float32)
    scaled = (wide * attention_norm_gain).astype(jnp.bfloat16)
    squares = jnp.sum(wide * wide, axis=1)
    part_qa = jnp.dot(scaled, query_first, preferred_element_type=jnp.float32)
    part_qb = jnp.dot(scaled, query_second, preferred_element_type=jnp.float32)
    part_ka = jnp.dot(scaled, key_first, preferred_element_type=jnp.float32)
    part_kb = jnp.dot(scaled, key_second, preferred_element_type=jnp.float32)
    part_value = jnp.dot(scaled, value_weight, preferred_element_type=jnp.float32)
    summed = packed_total((part_qa, part_qb, part_ka, part_kb, part_value, squares), "kv")
    factor = lax.rsqrt(summed[5] / D + EPS)[:, None]
    query_one = (summed[0] * factor).astype(jnp.bfloat16).reshape(batch, kv_local, group, HEAD_DIM)
    query_two = (summed[1] * factor).astype(jnp.bfloat16).reshape(batch, kv_local, group, HEAD_DIM)
    key_one = (summed[2] * factor).astype(jnp.bfloat16).reshape(batch, kv_local, HEAD_DIM)
    key_two = (summed[3] * factor).astype(jnp.bfloat16).reshape(batch, kv_local, HEAD_DIM)
    value_new = (summed[4] * factor).astype(jnp.bfloat16).reshape(batch, kv_local, 2 * HEAD_DIM)
    incoming_key_pair = jnp.concatenate([key_one, key_two], axis=2)
    is_last = lax.axis_index("kv") == lax.axis_size("kv") - 1
    fresh_values = value_new.astype(jnp.float32)[:, :, None, :]
    states = []
    for which, current_query, incoming_key in ((0, query_one, key_one), (1, query_two, key_two)):
        cached = key_cache[:, :, :, which * HEAD_DIM : (which + 1) * HEAD_DIM]
        scores = (
            jnp.einsum("bkgd,bckd->bkgc", current_query, cached, preferred_element_type=jnp.float32)
            * scale
        )
        fresh = (
            jnp.einsum(
                "fqsu,fqu->fqs", current_query, incoming_key, preferred_element_type=jnp.float32
            )
            * scale
        )
        fresh = jnp.where(is_last, fresh, -jnp.inf)
        top = jnp.maximum(jnp.max(scores, axis=3), fresh)
        expo = jnp.exp(scores - top[..., None])
        fresh_expo = jnp.exp(fresh - top)
        total = jnp.sum(expo, axis=3) + fresh_expo
        weighted = jnp.einsum(
            "bkgc,bckv->bkgv",
            expo.astype(jnp.bfloat16),
            value_cache,
            preferred_element_type=jnp.float32,
        )
        fresh_rounded = lax.optimization_barrier(fresh_expo.astype(jnp.bfloat16)).astype(
            jnp.float32
        )
        weighted = weighted + fresh_rounded[..., None] * fresh_values
        states.extend([top.reshape(-1), total.reshape(-1), weighted.reshape(-1, 2 * HEAD_DIM)])
    lam_rows = jnp.tile(lambdas, batch)
    pieces = (
        lax.all_to_all(states[0][None], "kv", split_axis=1, concat_axis=0, tiled=True),
        *side_by_side(
            (states[1][None], states[2][None], states[3][None], states[4][None], states[5][None]),
            "kv",
            1,
            0,
            2,
        ),
    )
    merged = source_positions(pieces)
    count = lam_rows.shape[0] // lax.axis_size("kv")
    lam_part = lax.dynamic_slice_in_dim(lam_rows, lax.axis_index("kv") * count, count)
    head_rows = collect(finish(merged, lam_part, head_gain), "kv", 0)
    heads_out = head_rows.reshape(batch, head_local * 2 * HEAD_DIM)
    attn_part = jnp.dot(heads_out, out_weight, preferred_element_type=jnp.float32)
    attn = summed_on_arrival(attn_part.astype(jnp.bfloat16), "tp", 1).astype(jnp.bfloat16)
    middle = (tokens.astype(jnp.float32) + attn.astype(jnp.float32)).astype(jnp.bfloat16)
    mid_block = collect(middle, "tp", 1)
    wide_mid = mid_block.astype(jnp.float32)
    scaled_mid = (wide_mid * mlp_gain).astype(jnp.bfloat16)
    squares_mid = jnp.sum(wide_mid * wide_mid, axis=1)
    gate_part = jnp.dot(scaled_mid, gate_weight, preferred_element_type=jnp.float32)
    up_part = jnp.dot(scaled_mid, up_weight, preferred_element_type=jnp.float32)
    gate_sum, up_sum, norm_sum = packed_total((gate_part, up_part, squares_mid), "kv")
    factor_mid = lax.rsqrt(norm_sum / D + EPS)[:, None]
    hidden = (jax.nn.silu(gate_sum * factor_mid) * (up_sum * factor_mid)).astype(jnp.bfloat16)
    down_part = jnp.dot(hidden, down_projection_weight, preferred_element_type=jnp.float32)
    feed = summed_on_arrival(down_part.astype(jnp.bfloat16), "tp", 1).astype(jnp.bfloat16)
    layer_out = (middle.astype(jnp.float32) + feed.astype(jnp.float32)).astype(jnp.bfloat16)
    return (layer_out, incoming_key_pair, value_new)


def solution(mesh):
    in_specs = (
        P(None, ("kv", "tp")),
        P("kv"),
        P("kv", "tp"),
        P("kv", "tp"),
        P("kv", "tp"),
        P("kv", "tp"),
        P("kv", "tp"),
        P(None, "kv", "tp", None),
        P(None, "kv", "tp", None),
        P("tp"),
        P(),
        P("tp", "kv"),
        P("kv"),
        P("kv", "tp"),
        P("kv", "tp"),
        P("tp", "kv"),
    )
    out_specs = (P(None, ("kv", "tp")), P(None, "tp", None), P(None, "tp", None))
    return jax.shard_map(shards, mesh=mesh, in_specs=in_specs, out_specs=out_specs, check_vma=False)
```

profile of v0, /device:TPU:1, one launch (start us, length us, event | category | flops | bytes accessed | tf_op | source)
XLA Modules:
  0.0 176.2 jit_solution(6454436221718843225)
XLA Ops:
  0.6 0.7 broadcast_bitcast_fusion.1
  1.5 10.2 %all_to_all.83 = bf16[8,2,256]{2,1,0:T(2,128)(2,1)S(1)} all-to-all(bf16[8,2,256]{2,1,0:T(2,128)(2,1)S(1)} %reshape.419), channel_id=1, replica_groups=mesh['kv'=32,'tp'=8] {'tp'}, dimensions={0} | all-to-all | bytes 16384 | tf_op jit(solution)/shard_map/all_to_all | solution.py:17
  11.8 0.7 fusion.36
  12.5 0.9 fusion.72
  13.5 0.9 fusion.71
  14.5 1.0 convolution_bitcast_fusion
  15.5 1.0 convolution_bitcast_fusion.1
  16.6 0.9 fusion.22
  17.5 0.2 all_to_all.57
  17.8 20.2 %all_to_all.84 = f32[32,1,769]{2,1,0:T(1,128)S(1)} all-to-all(f32[32,1,769]{2,1,0:T(1,128)S(1)} %all_to_all.57), channel_id=1, replica_groups=mesh['kv'=32,'tp'=8] {'kv'}, dimensions={0} | all-to-all | bytes 196864 | tf_op jit(solution)/shard_map/all_to_all | solution.py:45
  38.1 0.7 broadcast_in_dim.16
  38.8 3.9 %all-to-all-start.2 = ((f32[32,1,769]{2,1,0:T(1,128)}), f32[32,1,769]{2,1,0:T(1,128)S(1)}, u32[]{:S(2)}, u32[]{:S(2)}) async-start(f32[32,1,769]{2,1,0:T(1,128)} %broadcast_in_dim.16), calls=%async_computation.2 | async-start | bytes 229376 | tf_op jit(solution)/shard_map/all_to_all | solution.py:17
  42.7 9.3 %all-to-all-done.2 = f32[32,1,769]{2,1,0:T(1,128)S(1)} async-done(((f32[32,1,769]{2,1,0:T(1,128)}), f32[32,1,769]{2,1,0:T(1,128)S(1)}, u32[]{:S(2)}, u32[]{:S(2)}) %all-to-all-start.2) | async-done | bytes 98464 | tf_op jit(solution)/shard_map/all_to_all | solution.py:17
  51.9 0.3 reduce.18
  52.2 0.1 reshape.386
  53.0 0.1 fusion.41
  53.1 3.8 %fusion.70 = (f32[32,4]{1,0:T(8,128)S(1)}, f32[32,4,512]{2,1,0:T(4,128)S(1)}) fusion(bf16[32,4,64]{2,1,0:T(4,128)(2,1)S(1)} %get-tuple-element.27, bf16[32,512,1,128]{3,1,2,0:T(8,128)(2,1)} %param.23), kind=kOutput, calls=%fused_computation.107 | convolution fusion | flops 8519552 | bytes 4473344 | tf_op jit(solution)/shard_map/bkgd,bckd->bkgc/dot_general | solution.py:146
  56.9 1.3 fusion.69
  58.2 0.2 fusion.43
  58.3 0.6 fusion.45
  59.0 3.8 %all-to-all-start.4 = ((f32[1,32,4]{2,0,1:T(1,128)}), f32[1,32,4]{2,0,1:T(1,128)S(1)}, u32[]{:S(2)}, u32[]{:S(2)}) async-start(f32[1,32,4]{2,0,1:T(1,128)} %bitcast.39), calls=%async_computation.4 | async-start | bytes 32768 | tf_op jit(solution)/shard_map/all_to_all | solution.py:173
  62.8 1.0 fusion.24
  64.0 0.2 fusion.26
  64.4 3.1 %fusion.16 = f32[32,4,128]{2,1,0:T(4,128)S(1)} fusion(bf16[32,512,1,128]{3,1,2,0:T(8,128)(2,1)} %param.24, f32[32,4,512]{2,1,0:T(4,128)S(1)} %get-tuple-element.30, f32[32,4]{1,0:T(8,128)} %fusion.45, f32[32,128]{1,0:T(8,128)S(1)} %fusion.49, f32[32,4]{1,0:T(8,128)S(1)} %copy.124), kind=kOutput, calls=%fused_computation.12 | convolution fusion | flops 16941056 | bytes 4539392 | tf_op jit(solution)/shard_map/bkgc,bckv->bkgv/dot_general | solution.py:160
  67.5 0.4 copy-done.2
  67.9 0.7 fusion.19
  68.7 0.2 reshape_broadcast_in_dim_reshape.13
  68.8 0.1 reshape_broadcast_in_dim_reshape.14
  69.0 0.1 reshape_broadcast_in_dim_reshape.12
  69.1 1.6 concatenate.13
  70.7 0.7 all-to-all-done.4
  71.4 8.5 %all-to-all-start.3 = ((f32[1,128,259]{2,0,1:T(1,128)}), f32[1,128,259]{2,0,1:T(1,128)S(1)}, u32[]{:S(2)}, u32[]{:S(2)}) async-start(f32[1,128,259]{2,0,1:T(1,128)} %concatenate.13), calls=%async_computation.3 | async-start | bytes 393216 | tf_op jit(solution)/shard_map/all_to_all | solution.py:69
  80.3 9.6 %all-to-all-done.3 = f32[1,128,259]{2,0,1:T(1,128)S(1)} async-done(((f32[1,128,259]{2,0,1:T(1,128)}), f32[1,128,259]{2,0,1:T(1,128)S(1)}, u32[]{:S(2)}, u32[]{:S(2)}) %all-to-all-start.3) | async-done | bytes 132640 | tf_op jit(solution)/shard_map/all_to_all | solution.py:69
  89.8 0.5 reduce.19
  90.4 0.2 fusion.66
  90.7 0.1 copy.155
  90.9 0.2 fusion.56
  91.3 0.2 fusion.57
  91.6 0.2 fusion.33
  91.8 0.2 multiply_reduce_fusion.2
  92.1 12.0 %all_to_all.85 = bf16[32,4,128]{2,1,0:T(4,128)(2,1)S(1)} all-to-all(bf16[32,4,128]{2,1,0:T(4,128)(2,1)S(1)} %broadcast_in_dim.18), channel_id=1, replica_groups=mesh['kv'=32,'tp'=8] {'kv'}, dimensions={0} | all-to-all | bytes 65536 | tf_op jit(solution)/shard_map/all_to_all | solution.py:17
  104.1 0.1 convolution_convert_fusion
  104.2 0.1 copy.141
  104.3 0.1 reshape.421
  104.4 13.2 %all_to_all.86 = bf16[8,2,256]{2,1,0:T(2,128)(2,1)S(1)} all-to-all(bf16[8,2,256]{2,1,0:T(2,128)(2,1)S(1)} %reshape.421), channel_id=1, replica_groups=mesh['kv'=32,'tp'=8] {'tp'}, dimensions={0} | all-to-all | bytes 16384 | tf_op jit(solution)/shard_map/all_to_all | solution.py:76
  117.9 7.7 %all_to_all.87 = bf16[8,2,256]{2,1,0:T(2,128)(2,1)S(1)} all-to-all(bf16[8,2,256]{2,1,0:T(2,128)(2,1)S(1)} %reshape.423), channel_id=1, replica_groups=mesh['kv'=32,'tp'=8] {'tp'}, dimensions={0} | all-to-all | bytes 16384 | tf_op jit(solution)/shard_map/all_to_all | solution.py:17
  125.8 0.2 fusion.74
  126.0 0.2 fusion.73
  126.3 0.5 all_to_all.68
  126.8 16.5 %all_to_all.88 = f32[32,1,2817]{2,1,0:T(1,128)S(1)} all-to-all(f32[32,1,2817]{2,1,0:T(1,128)S(1)} %all_to_all.68), channel_id=1, replica_groups=mesh['kv'=32,'tp'=8] {'kv'}, dimensions={0} | all-to-all | bytes 721152 | tf_op jit(solution)/shard_map/all_to_all | solution.py:45
  143.4 0.2 reduce_sum.134
  143.6 0.9 broadcast_in_dim.20
  144.5 4.9 %all-to-all-start.9 = ((f32[32,1,2817]{2,1,0:T(1,128)}), f32[32,1,2817]{2,1,0:T(1,128)S(1)}, u32[]{:S(2)}, u32[]{:S(2)}) async-start(f32[32,1,2817]{2,1,0:T(1,128)} %broadcast_in_dim.20), calls=%async_computation.9 | async-start | bytes 753664 | tf_op jit(solution)/shard_map/all_to_all | solution.py:17
  149.5 0.7 fusion.39
  150.3 11.7 %all-to-all-done.9 = f32[32,1,2817]{2,1,0:T(1,128)S(1)} async-done(((f32[32,1,2817]{2,1,0:T(1,128)}), f32[32,1,2817]{2,1,0:T(1,128)S(1)}, u32[]{:S(2)}, u32[]{:S(2)}) %all-to-all-start.9) | async-done | bytes 360608 | tf_op jit(solution)/shard_map/all_to_all | solution.py:17
  162.0 0.9 reduce.20
  162.9 0.2 reshape.401
  163.2 0.3 convolution_convert_fusion.1
  163.5 0.1 copy.143
  163.6 0.7 reshape.425
  164.3 6.5 %all-to-all-start.10 = ((bf16[8,2,256]{2,1,0:T(2,128)(2,1)}), bf16[8,2,256]{2,1,0:T(2,128)(2,1)S(1)}, u32[]{:S(2)}, u32[]{:S(2)}) async-start(bf16[8,2,256]{2,1,0:T(2,128)(2,1)} %reshape.425), calls=%async_computation.10 | async-start | bytes 16384 | tf_op jit(solution)/shard_map/all_to_all | solution.py:76
  170.9 0.7 pad_maximum_fusion.1
  171.5 4.0 %all-to-all-done.10 = bf16[8,2,256]{2,1,0:T(2,128)(2,1)S(1)} async-done(((bf16[8,2,256]{2,1,0:T(2,128)(2,1)}), bf16[8,2,256]{2,1,0:T(2,128)(2,1)S(1)}, u32[]{:S(2)}, u32[]{:S(2)}) %all-to-all-start.10) | async-done | bytes 8224 | tf_op jit(solution)/shard_map/all_to_all | solution.py:76
  175.6 0.6 add_convert_fusion
  (84 shorter events, 3.4 us)
Async XLA Ops:
  0.6 125.1 %copy-start = (bf16[128,1408]{1,0:T(8,128)(2,1)S(1)}, bf16[128,1408]{1,0:T(8,128)(2,1)}, u32[]{:S(2)}) copy-start(bf16[128,1408]{1,0:T(8,128)(2,1)} %param.30) | copy-start | bytes 1081348
  38.8 13.1 %all-to-all-start.2 = ((f32[32,1,769]{2,1,0:T(1,128)}), f32[32,1,769]{2,1,0:T(1,128)S(1)}, u32[]{:S(2)}, u32[]{:S(2)}) async-start(f32[32,1,769]{2,1,0:T(1,128)} %broadcast_in_dim.16), calls=%async_computation.2 | async-start | bytes 229376 | tf_op jit(solution)/shard_map/all_to_all | solution.py:17
  52.8 4.1 %copy-start.1 = (bf16[32,512,1,128]{3,1,2,0:T(8,128)(2,1)S(1)}, bf16[32,512,1,128]{3,1,2,0:T(8,128)(2,1)}, u32[]{:S(2)}) copy-start(bf16[32,512,1,128]{3,1,2,0:T(8,128)(2,1)} %param.23) | copy-start | bytes 12582916
  59.0 12.5 %all-to-all-start.4 = ((f32[1,32,4]{2,0,1:T(1,128)}), f32[1,32,4]{2,0,1:T(1,128)S(1)}, u32[]{:S(2)}, u32[]{:S(2)}) async-start(f32[1,32,4]{2,0,1:T(1,128)} %bitcast.39), calls=%async_computation.4 | async-start | bytes 32768 | tf_op jit(solution)/shard_map/all_to_all | solution.py:173
  64.4 3.5 %copy-start.2 = (bf16[32,512,1,128]{3,1,2,0:T(8,128)(2,1)S(1)}, bf16[32,512,1,128]{3,1,2,0:T(8,128)(2,1)}, u32[]{:S(2)}) copy-start(bf16[32,512,1,128]{3,1,2,0:T(8,128)(2,1)} %param.24) | copy-start | bytes 12582916
  64.4 15.5 %copy-start.7 = (f32[4]{0:T(128)S(1)}, f32[4]{0:T(128)}, u32[]{:S(2)}) copy-start(f32[4]{0:T(128)} %param.25) | copy-start | bytes 52
  67.9 24.1 %copy-start.8 = (f32[128]{0:T(128)S(1)}, f32[128]{0:T(128)}, u32[]{:S(2)}) copy-start(f32[128]{0:T(128)} %param.26) | copy-start | bytes 1540
  67.9 36.2 %copy-start.4 = (bf16[512,128]{1,0:T(8,128)(2,1)S(1)}, bf16[512,128]{1,0:T(8,128)(2,1)}, u32[]{:S(2)}) copy-start(bf16[512,128]{1,0:T(8,128)(2,1)} %param.27) | copy-start | bytes 393220
  67.9 49.8 %copy-start.5 = (bf16[32,16]{0,1:T(8,128)(2,1)S(1)}, bf16[32,16]{0,1:T(8,128)(2,1)}, u32[]{:S(2)}) copy-start(bf16[32,16]{0,1:T(8,128)(2,1)} %param.16) | copy-start | bytes 3076
  67.9 57.7 %copy-start.6 = (f32[128]{0:T(128)S(1)}, f32[128]{0:T(128)}, u32[]{:S(2)}) copy-start(f32[128]{0:T(128)} %param.28) | copy-start | bytes 1540
  67.9 58.1 %copy-start.3 = (bf16[128,1408]{1,0:T(8,128)(2,1)S(1)}, bf16[128,1408]{1,0:T(8,128)(2,1)}, u32[]{:S(2)}) copy-start(bf16[128,1408]{1,0:T(8,128)(2,1)} %param.29) | copy-start | bytes 1081348
  71.4 18.4 %all-to-all-start.3 = ((f32[1,128,259]{2,0,1:T(1,128)}), f32[1,128,259]{2,0,1:T(1,128)S(1)}, u32[]{:S(2)}, u32[]{:S(2)}) async-start(f32[1,128,259]{2,0,1:T(1,128)} %concatenate.13), calls=%async_computation.3 | async-start | bytes 393216 | tf_op jit(solution)/shard_map/all_to_all | solution.py:69
  126.0 37.3 %copy-start.9 = (bf16[1408,128]{1,0:T(8,128)(2,1)S(1)}, bf16[1408,128]{1,0:T(8,128)(2,1)}, u32[]{:S(2)}) copy-start(bf16[1408,128]{1,0:T(8,128)(2,1)} %param.31) | copy-start | bytes 1081348
  144.5 17.5 %all-to-all-start.9 = ((f32[32,1,2817]{2,1,0:T(1,128)}), f32[32,1,2817]{2,1,0:T(1,128)S(1)}, u32[]{:S(2)}, u32[]{:S(2)}) async-start(f32[32,1,2817]{2,1,0:T(1,128)} %broadcast_in_dim.20), calls=%async_computation.9 | async-start | bytes 753664 | tf_op jit(solution)/shard_map/all_to_all | solution.py:17
  164.3 11.2 %all-to-all-start.10 = ((bf16[8,2,256]{2,1,0:T(2,128)(2,1)}), bf16[8,2,256]{2,1,0:T(2,128)(2,1)S(1)}, u32[]{:S(2)}, u32[]{:S(2)}) async-start(bf16[8,2,256]{2,1,0:T(2,128)(2,1)} %reshape.425), calls=%async_computation.10 | async-start | bytes 16384 | tf_op jit(solution)/shard_map/all_to_all | solution.py:76
where the time goes:
time: 177 us; the launch traced here: 176 us
  blocking collectives  79.8 us (45%)
  waiting for transfers between devices  35.2 us (20%)
  starting transfers between devices  27.6 us (16%)
  matrix products  14.7 us (8%)
  local copies, waits for them, and re-layouts  9.5 us (5%)
  other arithmetic  8.27 us (5%)
    all_to_all x2, blocking collectives, sum_at_owner(): tiles = lax.all_to_all(in_blocks(x, dim, length), axis, 0, 0, tiled=True)  36.8 us
    all_to_all x3, blocking collectives, sent_to_all(): return lax.all_to_all(copies, axis, split_axis=0, concat_axis=0, tiled=True)  29.9 us
    all_to_all x2, waiting for transfers between devices, sent_to_all(): return lax.all_to_all(copies, axis, split_axis=0, concat_axis=0, tiled=True)  21 us
    all_to_all x1, blocking collectives, summed_on_arrival(): tiles = lax.all_to_all(in_blocks(x, dim, length), axis, 0, 0, tiled=True)  13.2 us
    all_to_all x1, waiting for transfers between devices, side_by_side(): lax.all_to_all(both, axis, split_axis=split_dim, concat_axis=concat_dim,...  9.57 us
    all_to_all x2, starting transfers between devices, sent_to_all(): return lax.all_to_all(copies, axis, split_axis=0, concat_axis=0, tiled=True)  8.71 us
    all_to_all x1, starting transfers between devices, side_by_side(): lax.all_to_all(both, axis, split_axis=split_dim, concat_axis=concat_dim,...  8.51 us
    all_to_all x1, starting transfers between devices, summed_on_arrival(): tiles = lax.all_to_all(in_blocks(x, dim, length), axis, 0, 0, tiled=True)  6.54 us
  transfers between devices with their start and end apart: 5, of which 5 were waited for; matrix products, arithmetic and copies ran while one was open for 5% of the time, Pallas kernels for 0%

commit v1 on v0

v1 whole, which is shorter than its diff:
```python
import functools

import jax
import jax.numpy as jnp
from jax import lax
from jax.experimental import pallas as pl
from jax.experimental.pallas import tpu as pltpu
from jax.sharding import PartitionSpec as P

D = 4096
HD = 64
EPS = 1e-06
NZ, NY = 8, 4
KV = NZ * NY
TP = 8
F32 = jnp.float32
BF16 = jnp.bfloat16
MESH = pl.DeviceIdType.MESH

Z_DIST = [min(k, NZ - k) for k in range(NZ)]
Y_DIST = [min(k, NY - k) for k in range(NY)]
OFFSETS = sorted(
    [(dz, dy) for dz in range(NZ) for dy in range(NY) if (dz, dy) != (0, 0)],
    key=lambda o: -(Z_DIST[o[0]] + Y_DIST[o[1]]),
)


def kernel(
    tok_h, an_gain_h, wq1_h, wq2_h, wk1_h, wk2_h, wv_h, k_h, v_h, lam_h, hg_h, wo_h, mg_h, wg_h,
    wu_h, wd_h,
    out_ref, kp_ref, nv_ref,
    an_gain, wq1, wq2, wq, wk, wv, keys, vals, lam, hg, wo, mg, wg, wu, wd,
    tok, b1_s, b1_r, b2_s, b2_r, c1_s, c1_r, c2_s, c2_r, c2_f, d_s, d_r, e1_f, e1_s, e1_r, e2_s,
    e2_r, e2_f, mid_t, f_s, f_r,
    ld, tok_ss, tok_rs, b1_ss, b1_rs, b2_ss, b2_rs, c1_ss, c1_rs, c2_ss, c2_rs, d_ss, d_rs,
    e1_ss, e1_rs, e2_ss, e2_rs, f_ss, f_rs,
):
    kv = lax.axis_index("kv")
    tp = lax.axis_index("tp")
    mz, my = kv // NY, kv % NY

    def kv_peer(dz, dy):
        return ((mz + dz) % NZ) * NY + (my + dy) % NY

    def tp_peer(k):
        return (tp + k) % TP

    loads = []

    def load(src, dst):
        copy = pltpu.make_async_copy(src, dst, ld.at[len(loads)])
        copy.start()
        loads.append(copy)
        return copy

    l_tok = load(tok_h, tok.at[tp])
    l_ag = load(an_gain_h, an_gain)
    l_w = [
        load(wq1_h, wq1), load(wq2_h, wq2), load(wk1_h, wk.at[pl.ds(0, HD)]),
        load(wk2_h, wk.at[pl.ds(HD, HD)]), load(wv_h, wv),
    ]

    barrier = pltpu.get_barrier_semaphore()
    for dz, dy in OFFSETS:
        pl.semaphore_signal(barrier, inc=1, device_id=(kv_peer(dz, dy), tp), device_id_type=MESH)
    for k in range(1, TP):
        pl.semaphore_signal(barrier, inc=1, device_id=(kv, tp_peer(k)), device_id_type=MESH)

    l_k = [load(k_h.at[pl.ds(8 * i, 8)], keys.at[pl.ds(8 * i, 8)]) for i in range(4)]
    l_v = [load(v_h.at[pl.ds(8 * i, 8)], vals.at[pl.ds(8 * i, 8)]) for i in range(4)]
    l_lam = load(lam_h, lam)
    l_hg = load(hg_h, hg)
    l_wo = load(wo_h, wo)
    l_mg = load(mg_h, mg)
    l_gu = [load(wg_h, wg), load(wu_h, wu)]
    l_wd = load(wd_h, wd)

    def send(src, dst, ss, rs, device):
        copy = pltpu.make_async_remote_copy(
            src_ref=src, dst_ref=dst, send_sem=ss, recv_sem=rs, device_id=device,
            device_id_type=MESH,
        )
        copy.start()

    def all_in(ref, sem):
        pltpu.make_async_copy(ref, ref, sem).wait()

    for c in l_w:
        c.wait()
    for h in range(4):
        wq[:, 128 * h : 128 * h + 128] = jnp.concatenate(
            [wq1[:, HD * h : HD * h + HD], wq2[:, HD * h : HD * h + HD]], axis=1
        )
    b1_s[...] = jnp.zeros_like(b1_s)
    e1_f[...] = jnp.zeros_like(e1_f)
    l_tok.wait()
    l_ag.wait()
    pl.semaphore_wait(barrier, KV - 1 + TP - 1)

    for k in (4, 5, 3, 2, 6, 7, 1):
        send(tok.at[tp], tok.at[tp], tok_ss, tok_rs, (kv, tp_peer(k)))
    all_in(tok.at[pl.ds(0, TP - 1)], tok_rs)
    x = tok[...].astype(F32).reshape(TP * 16, KV).T
    scaled = (x * an_gain[...]).astype(BF16)
    sq = jnp.sum(x * x, axis=1, keepdims=True)
    b1_s[pl.ds(6, KV, stride=8), :] = jnp.broadcast_to(sq, (KV, 128))
    pq = jnp.dot(scaled, wq[...], preferred_element_type=F32)
    for h in range(4):
        b1_s[pl.ds(h, KV, stride=8), :] = pq[:, 128 * h : 128 * h + 128]
    b1_s[pl.ds(4, KV, stride=8), :] = lax.dot_general(
        scaled, wk[...], (((1,), (1,)), ((), ())), preferred_element_type=F32
    )
    b1_s[pl.ds(5, KV, stride=8), :] = jnp.dot(scaled, wv[...], preferred_element_type=F32)

    def rows(ref, i, n):
        return ref.at[pl.ds(pl.multiple_of(i * n, n), n)]

    for dz, dy in OFFSETS:
        p = kv_peer(dz, dy)
        send(rows(b1_s, p, 8), rows(b1_r, kv, 8), b1_ss, b1_rs, (p, tp))
    own = pl.ds(pl.multiple_of(kv * 8, 8), 8)
    b1_r[own, :] = b1_s[own, :]
    all_in(b1_r.at[pl.ds(0, (KV - 1) * 8)], b1_rs)
    total = jnp.sum(b1_r[...].reshape(KV, 8, 128), axis=0)
    factor = lax.rsqrt(total[6:7] / D + EPS)
    proj = (total * factor).astype(BF16).astype(F32)
    lane = lax.broadcasted_iota(jnp.int32, (8, 128), 1)
    row = lax.broadcasted_iota(jnp.int32, (8, 128), 0)
    both = jnp.concatenate([proj[0:4], proj[0:4]], axis=0)
    query = jnp.where((lane < HD) == (row < 4), both, 0.0)
    b2_s[...] = query.astype(BF16)

    for dz, dy in OFFSETS:
        send(b2_s, b2_r.at[kv], b2_ss, b2_rs.at[kv], (kv_peer(dz, dy), tp))
    b2_r[kv] = query.astype(BF16)
    scale = HD ** (-0.5)
    new_key, new_value = proj[4:5], proj[5:6]
    fresh = jnp.sum(query * new_key, axis=1, keepdims=True) * scale

    for c in l_k + l_v:
        c.wait()

    def attend(g, carry):
        half = (g + 1) // 2
        dz = (g % 2) * half + (1 - g % 2) * ((NZ - half) % NZ)
        base = ((mz + dz) % NZ) * NY
        for j in range(NY):
            s = base + j

            @pl.when(s != kv)
            def _():
                pltpu.make_async_copy(b2_r.at[s], b2_r.at[s], b2_rs.at[s]).wait()

        lane16 = lax.broadcasted_iota(jnp.int32, (8, 128), 1)
        for j in range(NY):
            s = base + j
            score = (
                lax.dot_general(
                    b2_r[s], keys[s], (((1,), (1,)), ((), ())), preferred_element_type=F32
                )
                * scale
            )
            top = jnp.max(score, axis=1, keepdims=True)
            expo = jnp.exp(score - top)
            tot = jnp.sum(expo, axis=1, keepdims=True)
            value = jnp.dot(expo.astype(BF16), vals[s], preferred_element_type=F32) / tot
            level = jnp.broadcast_to(top + jnp.log(tot), (8, 128))
            p1 = level.astype(BF16).astype(F32)
            p2 = (level - p1).astype(BF16).astype(F32)
            p3 = level - p1 - p2
            pieces = jnp.where(
                lane16 == 0, p1, jnp.where(lane16 == 1, p2, jnp.where(lane16 == 2, p3, 0.0))
            )
            c1_s[s] = jnp.concatenate([value, pieces], axis=0).astype(BF16)
        for j in range(NY):
            s = base + j

            @pl.when(s != kv)
            def _():
                send(c1_s.at[s], c1_r.at[kv], c1_ss, c1_rs, (s, tp))

        return carry

    lax.fori_loop(0, NZ, attend, 0)
    c1_r[kv] = c1_s[kv]

    for c in (l_lam, l_hg, l_wo, l_mg):
        c.wait()
    r4 = lax.broadcasted_iota(jnp.int32, (4, 128), 0)
    lam_rows = jnp.where(
        r4 == 0, lam[0], jnp.where(r4 == 1, lam[1], jnp.where(r4 == 2, lam[2], lam[3]))
    )
    all_in(c1_r.at[pl.ds(0, KV - 1)], c1_rs)
    states = c1_r[...].astype(F32)
    values = states[:, 0:8, :]
    levels = jnp.sum(states[:, 8:16, :], axis=2, keepdims=True)
    top = jnp.maximum(jnp.max(levels, axis=0), fresh)
    weight = jnp.exp(levels - top[None])
    fresh_weight = jnp.exp(fresh - top)
    total_w = jnp.sum(weight, axis=0) + fresh_weight
    merged = (jnp.sum(values * weight, axis=0) + fresh_weight * new_value) / total_w
    mixed = merged[0:4] - lam_rows * merged[4:8]
    normed = (
        mixed * lax.rsqrt(jnp.mean(mixed * mixed, axis=1, keepdims=True) + EPS) * hg[...]
    )
    c2 = jnp.concatenate([normed, proj[4:6], jnp.zeros((2, 128), F32)], axis=0).astype(BF16)
    c2_s[...] = c2

    for dz, dy in OFFSETS:
        send(c2_s, c2_r.at[kv], c2_ss, c2_rs, (kv_peer(dz, dy), tp))
    c2_r[kv] = c2
    all_in(c2_r.at[pl.ds(0, KV - 1)], c2_rs)
    c2_f[...] = c2_r[...].astype(F32).reshape(KV * 8, 128)
    heads = jnp.concatenate(
        [c2_f[pl.ds(h, KV, stride=8), :].astype(BF16) for h in range(4)], axis=1
    )
    attn_part = jnp.dot(heads, wo[...], preferred_element_type=F32).astype(BF16)
    d_s[...] = attn_part

    for k in (4, 5, 3, 2, 6, 7, 1):
        send(d_s, d_r.at[tp], d_ss, d_rs, (kv, tp_peer(k)))
    d_r[tp] = attn_part
    kp_ref[...] = c2_f[pl.ds(4, KV, stride=8), :].astype(BF16)
    nv_ref[...] = c2_f[pl.ds(5, KV, stride=8), :].astype(BF16)
    all_in(d_r.at[pl.ds(0, TP - 1)], d_rs)
    attn = jnp.sum(d_r[...].astype(F32), axis=0).astype(BF16).astype(F32)
    middle = (x + attn).astype(BF16).astype(F32)
    scaled_mid = (middle * mg[...]).astype(BF16)
    sq_mid = jnp.broadcast_to(jnp.sum(middle * middle, axis=1, keepdims=True), (KV, 128))
    for c in l_gu:
        c.wait()
    lane32 = lax.broadcasted_iota(jnp.int32, (KV, 128), 1)
    s1 = sq_mid.astype(BF16).astype(F32)
    s2 = (sq_mid - s1).astype(BF16).astype(F32)
    e1_f[pl.ds(22, KV, stride=24), :] = jnp.where(
        lane32 == 0, s1, jnp.where(lane32 == 1, s2, jnp.where(lane32 == 2, sq_mid - s1 - s2, 0.0))
    )
    gate = jnp.dot(scaled_mid, wg[...], preferred_element_type=F32)
    for c in range(11):
        e1_f[pl.ds(c, KV, stride=24), :] = gate[:, 128 * c : 128 * c + 128]
    up = jnp.dot(scaled_mid, wu[...], preferred_element_type=F32)
    for c in range(11):
        e1_f[pl.ds(11 + c, KV, stride=24), :] = up[:, 128 * c : 128 * c + 128]
    e1_s[...] = e1_f[...].reshape(KV * 3, 8, 128).astype(BF16)

    def thirds(ref, i):
        return ref.at[pl.ds(i * 3, 3)]

    for dz, dy in OFFSETS:
        p = kv_peer(dz, dy)
        send(thirds(e1_s, p), thirds(e1_r, kv), e1_ss, e1_rs, (p, tp))
    e1_r[pl.ds(kv * 3, 3)] = e1_s[pl.ds(kv * 3, 3)]
    mid_t[...] = middle.T.reshape(TP, 16, KV)
    all_in(e1_r.at[pl.ds(0, (KV - 1) * 3)], e1_rs)
    sums = jnp.sum(e1_r[...].astype(F32).reshape(KV, 24, 128), axis=0)
    factor_mid = lax.rsqrt(jnp.sum(sums[22:23], axis=1, keepdims=True) / D + EPS)
    gate_all = sums[0:11] * factor_mid
    up_all = sums[11:22] * factor_mid
    hidden = gate_all / (1.0 + jnp.exp(-gate_all)) * up_all
    hidden = jnp.concatenate([hidden, jnp.zeros((5, 128), F32)], axis=0).astype(BF16)
    e2_s[...] = hidden

    for dz, dy in OFFSETS:
        send(e2_s, e2_r.at[kv], e2_ss, e2_rs, (kv_peer(dz, dy), tp))
    e2_r[kv] = hidden
    l_wd.wait()
    all_in(e2_r.at[pl.ds(0, KV - 1)], e2_rs)
    e2_f[...] = e2_r[...].astype(F32).reshape(KV * 16, 128)
    hid = jnp.concatenate(
        [e2_f[pl.ds(c, KV, stride=16), :].astype(BF16) for c in range(11)], axis=1
    )
    down = jnp.dot(hid, wd[...], preferred_element_type=F32)
    f_s[...] = down.T.astype(BF16).reshape(TP, 16, KV)

    for k in (4, 5, 3, 2, 6, 7, 1):
        p = tp_peer(k)
        send(f_s.at[p], f_r.at[tp], f_ss, f_rs, (kv, p))
    f_r[tp] = f_s[tp]
    all_in(f_r.at[pl.ds(0, TP - 1)], f_rs)
    feed = jnp.sum(f_r[...].astype(F32), axis=0).astype(BF16).astype(F32)
    out_ref[...] = (mid_t[tp] + feed).astype(BF16)

    def all_out(ref, sem):
        pltpu.make_async_copy(ref, ref, sem).wait()

    all_out(tok.at[pl.ds(0, TP - 1)], tok_ss)
    all_out(b1_s.at[pl.ds(0, (KV - 1) * 8)], b1_ss)
    all_out(b2_r.at[pl.ds(0, KV - 1)], b2_ss)
    all_out(c1_s.at[pl.ds(0, KV - 1)], c1_ss)
    all_out(c2_r.at[pl.ds(0, KV - 1)], c2_ss)
    all_out(d_r.at[pl.ds(0, TP - 1)], d_ss)
    all_out(e1_s.at[pl.ds(0, (KV - 1) * 3)], e1_ss)
    all_out(e2_r.at[pl.ds(0, KV - 1)], e2_ss)
    all_out(f_s.at[pl.ds(0, TP - 1)], f_ss)


def shards(
    tokens, attention_norm_gain, query_first, query_second, key_first, key_second, value_weight,
    key_cache, value_cache, lambdas, head_gain, out_weight, mlp_gain, gate_weight, up_weight,
    down_projection_weight,
):
    hbm = pl.BlockSpec(memory_space=pl.ANY)
    vmem = pl.BlockSpec(memory_space=pltpu.VMEM)
    dma = pltpu.SemaphoreType.DMA
    out, kp, nv = pl.pallas_call(
        kernel,
        out_shape=(
            jax.ShapeDtypeStruct((16, KV), BF16),
            jax.ShapeDtypeStruct((KV, 128), BF16),
            jax.ShapeDtypeStruct((KV, 128), BF16),
        ),
        in_specs=[hbm] * 16,
        out_specs=(vmem, vmem, vmem),
        scratch_shapes=[
            pltpu.VMEM((1, 128), F32),
            pltpu.VMEM((128, 256), BF16),
            pltpu.VMEM((128, 256), BF16),
            pltpu.VMEM((128, 512), BF16),
            pltpu.VMEM((128, 128), BF16),
            pltpu.VMEM((128, 128), BF16),
            pltpu.VMEM((KV, 512, 128), BF16),
            pltpu.VMEM((KV, 512, 128), BF16),
            pltpu.SMEM((4,), F32),
            pltpu.VMEM((1, 128), F32),
            pltpu.VMEM((512, 128), BF16),
            pltpu.VMEM((1, 128), F32),
            pltpu.VMEM((128, 1408), BF16),
            pltpu.VMEM((128, 1408), BF16),
            pltpu.VMEM((1408, 128), BF16),
            pltpu.VMEM((TP, 16, KV), BF16),
            pltpu.VMEM((KV * 8, 128), F32),
            pltpu.VMEM((KV * 8, 128), F32),
            pltpu.VMEM((8, 128), BF16),
            pltpu.VMEM((KV, 8, 128), BF16),
            pltpu.VMEM((KV, 16, 128), BF16),
            pltpu.VMEM((KV, 16, 128), BF16),
            pltpu.VMEM((8, 128), BF16),
            pltpu.VMEM((KV, 8, 128), BF16),
            pltpu.VMEM((KV * 8, 128), F32),
            pltpu.VMEM((KV, 128), BF16),
            pltpu.VMEM((TP, KV, 128), BF16),
            pltpu.VMEM((KV * 24, 128), F32),
            pltpu.VMEM((KV * 3, 8, 128), BF16),
            pltpu.VMEM((KV * 3, 8, 128), BF16),
            pltpu.VMEM((16, 128), BF16),
            pltpu.VMEM((KV, 16, 128), BF16),
            pltpu.VMEM((KV * 16, 128), F32),
            pltpu.VMEM((TP, 16, KV), F32),
            pltpu.VMEM((TP, 16, KV), BF16),
            pltpu.VMEM((TP, 16, KV), BF16),
            dma((24,)),
            dma(()), dma(()), dma(()), dma(()), dma(()), dma((KV,)), dma(()), dma(()), dma(()),
            dma(()), dma(()), dma(()), dma(()), dma(()), dma(()), dma(()), dma(()), dma(()),
        ],
        compiler_params=pltpu.CompilerParams(collective_id=0, has_side_effects=True),
        name="decode_layer",
    )(
        tokens.T,
        attention_norm_gain.reshape(1, 128),
        query_first,
        query_second,
        key_first.T,
        key_second.T,
        value_weight,
        key_cache.reshape(KV, 512, 128),
        value_cache.reshape(KV, 512, 128),
        lambdas,
        head_gain.reshape(1, 128),
        out_weight,
        mlp_gain.reshape(1, 128),
        gate_weight,
        up_weight,
        down_projection_weight,
    )
    return out.T, kp[:, None, :], nv[:, None, :]


def solution(mesh):
    in_specs = (
        P(None, ("kv", "tp")),
        P("kv"),
        P("kv", "tp"),
        P("kv", "tp"),
        P("kv", "tp"),
        P("kv", "tp"),
        P("kv", "tp"),
        P(None, "kv", "tp", None),
        P(None, "kv", "tp", None),
        P("tp"),
        P(),
        P("tp", "kv"),
        P("kv"),
        P("kv", "tp"),
        P("kv", "tp"),
        P("tp", "kv"),
    )
    out_specs = (P(None, ("kv", "tp")), P(None, "tp", None), P(None, "tp", None))
    return jax.shard_map(shards, mesh=mesh, in_specs=in_specs, out_specs=out_specs, check_vma=False)
```

time: 177 us -> 73.2 us (0.41)
  blocking collectives: 79.8 us -> 0 us
  Pallas kernels: 0 us -> 68.4 us
  waiting for transfers between devices: 35.2 us -> 0 us
  starting transfers between devices: 27.6 us -> 0 us
  matrix products: 14.7 us -> 0 us
  other arithmetic: 8.27 us -> 0 us
  local copies, waits for them, and re-layouts: 9.5 us -> 3.86 us
    all_to_all x6 -> x0, blocking collectives: 79.8 us -> none  [the longest x2 36.8 us: sum_at_owner(): tiles = lax.all_to_all(in_blocks(x, dim, length), axis, 0, 0, tiled=True)]
    pallas_call x0 -> x1, Pallas kernels: none -> 68.4 us  [shards(): pl.pallas_call(kernel, out_shape=(jax.ShapeDtypeStruct((16, KV), BF16), j...]
    all_to_all x5 -> x0, waiting for transfers between devices: 35.2 us -> none  [the longest x2 21 us: sent_to_all(): return lax.all_to_all(copies, axis, split_axis=0, concat_axis=0, tiled=True)]
    all_to_all x5 -> x0, starting transfers between devices: 27.6 us -> none  [the longest x2 8.71 us: sent_to_all(): return lax.all_to_all(copies, axis, split_axis=0, concat_axis=0, tiled=True)]
    dot_general x15 -> x0, matrix products: 14.7 us -> none  [the longest x2 5.04 us: shards(): jnp.einsum('bkgd,bckd->bkgc', current_query, cached, preferred_element_ty...]
    convert_element_type x12 -> x0, other arithmetic: 2.52 us -> none  [the longest x1 0.74 us: shards(): scaled = (wide * attention_norm_gain).astype(jnp.bfloat16)]
    reduce_sum x12 -> x0, other arithmetic: 2.42 us -> none  [the longest x2 1.2 us: shards(): total = jnp.sum(expo, axis=3) + fresh_expo]
    unnamed x37 -> x3, local copies, waits for them, and re-layouts: 2.71 us -> 3.86 us
  transfers between devices with their start and end apart: 5 -> 0, of which waited for: 5 -> 0; matrix products, arithmetic and copies ran while one was open for 5% -> 0% of each run, Pallas kernels for 0% -> 0%
where the time goes in v1:
time: 73.2 us; the launch traced here: 72.9 us
  Pallas kernels  68.4 us (93%)
  local copies, waits for them, and re-layouts  3.86 us (5%)
    pallas_call x1, Pallas kernels, shards(): pl.pallas_call(kernel, out_shape=(jax.ShapeDtypeStruct((16, KV), BF16), j...  68.4 us
    unnamed x3, local copies, waits for them, and re-layouts  3.86 us

profile of v1, /device:TPU:1, one launch (start us, length us, event | category | flops | bytes accessed | tf_op | source)
XLA Modules:
  0.0 72.9 jit_solution(984208204421300906)
XLA Ops:
  0.6 68.4 %decode_layer.1 = (bf16[16,32]{1,0:T(8,128)(2,1)}, bf16[32,128]{1,0:T(8,128)(2,1)}, bf16[32,128]{1,0:T(8,128)(2,1)}) custom-call(bf16[16,32]{1,0:T(8,128)(2,1)} %bitcast.17, f32[1,128]{1,0:T(1,128)} %bitcast.19, bf16[128,256]{1,0:T(8,128)(2,1)} %wq1_h.1, bf16[128,256]{1,0:T(8,128)(2,1)} %wq2_h.1, bf16[64,128]{1,0:T(8,128)(2,1)} %bitcast.13, ...), custom_call_target="tpu_custom_call" | custom-call | tf_op jit(solution)/shard_map/decode_layer/pallas_call | solution.py:305
  69.0 1.3 %copy.22 = bf16[32,16]{0,1:T(8,128)(2,1)} copy(bf16[32,16]{0,1:T(8,128)(2,1)} %bitcast.18) | data formatting | bytes 2048
  70.3 1.3 %copy.23 = bf16[32,1,128]{2,0,1:T(8,128)(2,1)} copy(bf16[32,1,128]{2,0,1:T(8,128)(2,1)} %bitcast.16) | data formatting | bytes 16384
  71.6 1.3 %copy.24 = bf16[32,1,128]{2,0,1:T(8,128)(2,1)} copy(bf16[32,1,128]{2,0,1:T(8,128)(2,1)} %bitcast.15) | data formatting | bytes 16384

commit v2 on v1

--- a/solution.py
+++ b/solution.py
@@ -31,7 +31,7 @@
     out_ref, kp_ref, nv_ref,
     an_gain, wq1, wq2, wq, wk, wv, keys, vals, lam, hg, wo, mg, wg, wu, wd,
     tok, b1_s, b1_r, b2_s, b2_r, c1_s, c1_r, c2_s, c2_r, c2_f, d_s, d_r, e1_f, e1_s, e1_r, e2_s,
-    e2_r, e2_f, mid_t, f_s, f_r,
+    e2_r, e2_f, mid_t, f_s, f_r, keys_t, s_scr,
     ld, tok_ss, tok_rs, b1_ss, b1_rs, b2_ss, b2_rs, c1_ss, c1_rs, c2_ss, c2_rs, d_ss, d_rs,
     e1_ss, e1_rs, e2_ss, e2_rs, f_ss, f_rs,
 ):
@@ -120,6 +120,14 @@
         send(rows(b1_s, p, 8), rows(b1_r, kv, 8), b1_ss, b1_rs, (p, tp))
     own = pl.ds(pl.multiple_of(kv * 8, 8), 8)
     b1_r[own, :] = b1_s[own, :]
+    for c in l_k + l_v:
+        c.wait()
+
+    def turn(s, carry):
+        keys_t[s] = keys[s].T
+        return carry
+
+    lax.fori_loop(0, KV, turn, 0, unroll=2)
     all_in(b1_r.at[pl.ds(0, (KV - 1) * 8)], b1_rs)
     total = jnp.sum(b1_r[...].reshape(KV, 8, 128), axis=0)
     factor = lax.rsqrt(total[6:7] / D + EPS)
@@ -127,61 +135,76 @@
     lane = lax.broadcasted_iota(jnp.int32, (8, 128), 1)
     row = lax.broadcasted_iota(jnp.int32, (8, 128), 0)
     both = jnp.concatenate([proj[0:4], proj[0:4]], axis=0)
-    query = jnp.where((lane < HD) == (row < 4), both, 0.0)
+    query = jnp.where((lane < HD) == (row < 4), both, 0.0) * HD ** (-0.5)
     b2_s[...] = query.astype(BF16)
 
     for dz, dy in OFFSETS:
         send(b2_s, b2_r.at[kv], b2_ss, b2_rs.at[kv], (kv_peer(dz, dy), tp))
     b2_r[kv] = query.astype(BF16)
-    scale = HD ** (-0.5)
     new_key, new_value = proj[4:5], proj[5:6]
-    fresh = jnp.sum(query * new_key, axis=1, keepdims=True) * scale
-
-    for c in l_k + l_v:
-        c.wait()
-
-    def attend(g, carry):
+    fresh = jnp.sum(query * new_key, axis=1, keepdims=True)
+
+    def plane(g):
         half = (g + 1) // 2
         dz = (g % 2) * half + (1 - g % 2) * ((NZ - half) % NZ)
-        base = ((mz + dz) % NZ) * NY
+        return ((mz + dz) % NZ) * NY
+
+    def arrive(g):
         for j in range(NY):
-            s = base + j
+            s = plane(g) + j
 
             @pl.when(s != kv)
             def _():
                 pltpu.make_async_copy(b2_r.at[s], b2_r.at[s], b2_rs.at[s]).wait()
 
-        lane16 = lax.broadcasted_iota(jnp.int32, (8, 128), 1)
+    def scores(g):
+        return [
+            jnp.dot(b2_r[plane(g) + j], keys_t[plane(g) + j], preferred_element_type=F32)
+            for j in range(NY)
+        ]
+
+    def values(g, score):
+        top = [jnp.max(t, axis=1, keepdims=True) for t in score]
+        expo = [jnp.exp(t - m) for t, m in zip(score, top)]
+        acc = [
+            jnp.dot(e.astype(BF16), vals[plane(g) + j], preferred_element_type=F32)
+            for j, e in enumerate(expo)
+        ]
         for j in range(NY):
-            s = base + j
-            score = (
-                lax.dot_general(
-                    b2_r[s], keys[s], (((1,), (1,)), ((), ())), preferred_element_type=F32
-                )
-                * scale
-            )
-            top = jnp.max(score, axis=1, keepdims=True)
-            expo = jnp.exp(score - top)
-            tot = jnp.sum(expo, axis=1, keepdims=True)
-            value = jnp.dot(expo.astype(BF16), vals[s], preferred_element_type=F32) / tot
-            level = jnp.broadcast_to(top + jnp.log(tot), (8, 128))
+            tot = jnp.sum(expo[j], axis=1, keepdims=True)
+            level = jnp.broadcast_to(top[j] + jnp.log(tot), (8, 128))
             p1 = level.astype(BF16).astype(F32)
             p2 = (level - p1).astype(BF16).astype(F32)
             p3 = level - p1 - p2
             pieces = jnp.where(
-                lane16 == 0, p1, jnp.where(lane16 == 1, p2, jnp.where(lane16 == 2, p3, 0.0))
+                lane == 0, p1, jnp.where(lane == 1, p2, jnp.where(lane == 2, p3, 0.0))
             )
-            c1_s[s] = jnp.concatenate([value, pieces], axis=0).astype(BF16)
+            c1_s[plane(g) + j] = jnp.concatenate([acc[j] / tot, pieces], axis=0).astype(BF16)
+
+    def depart(g):
         for j in range(NY):
-            s = base + j
+            s = plane(g) + j
 
             @pl.when(s != kv)
             def _():
                 send(c1_s.at[s], c1_r.at[kv], c1_ss, c1_rs, (s, tp))
 
+    def attend(g, carry):
+        arrive(g)
+        before = [s_scr[(g + 1) % 2, j] for j in range(NY)]
+        now = scores(g)
+        values(g - 1, before)
+        for j in range(NY):
+            s_scr[g % 2, j] = now[j]
+        depart(g - 1)
         return carry
 
-    lax.fori_loop(0, NZ, attend, 0)
+    arrive(0)
+    for j, t in enumerate(scores(0)):
+        s_scr[0, j] = t
+    lax.fori_loop(1, NZ, attend, 0)
+    values(NZ - 1, [s_scr[(NZ - 1) % 2, j] for j in range(NY)])
+    depart(NZ - 1)
     c1_r[kv] = c1_s[kv]
 
     for c in (l_lam, l_hg, l_wo, l_mg):
@@ -294,20 +317,26 @@
     all_out(f_s.at[pl.ds(0, TP - 1)], f_ss)
 
 
+def hand_over(a_ref, b_ref, c_ref, x_ref, y_ref, z_ref):
+    x_ref[...] = a_ref[...]
+    y_ref[...] = b_ref[...]
+    z_ref[...] = c_ref[...]
+
+
 def shards(
     tokens, attention_norm_gain, query_first, query_second, key_first, key_second, value_weight,
     key_cache, value_cache, lambdas, head_gain, out_weight, mlp_gain, gate_weight, up_weight,
     down_projection_weight,
 ):
-    hbm = pl.BlockSpec(memory_space=pl.ANY)
+    hbm = pl.BlockSpec(memory_space=pltpu.HBM)
     vmem = pl.BlockSpec(memory_space=pltpu.VMEM)
     dma = pltpu.SemaphoreType.DMA
     out, kp, nv = pl.pallas_call(
         kernel,
         out_shape=(
-            jax.ShapeDtypeStruct((16, KV), BF16),
-            jax.ShapeDtypeStruct((KV, 128), BF16),
-            jax.ShapeDtypeStruct((KV, 128), BF16),
+            pltpu.VMEM((16, KV), BF16),
+            pltpu.VMEM((KV, 128), BF16),
+            pltpu.VMEM((KV, 128), BF16),
         ),
         in_specs=[hbm] * 16,
         out_specs=(vmem, vmem, vmem),
@@ -348,11 +377,15 @@
             pltpu.VMEM((TP, 16, KV), F32),
             pltpu.VMEM((TP, 16, KV), BF16),
             pltpu.VMEM((TP, 16, KV), BF16),
+            pltpu.VMEM((KV, 128, 512), BF16),
+            pltpu.VMEM((2, NY, 8, 512), F32),
             dma((24,)),
             dma(()), dma(()), dma(()), dma(()), dma(()), dma((KV,)), dma(()), dma(()), dma(()),
             dma(()), dma(()), dma(()), dma(()), dma(()), dma(()), dma(()), dma(()), dma(()),
         ],
-        compiler_params=pltpu.CompilerParams(collective_id=0, has_side_effects=True),
+        compiler_params=pltpu.CompilerParams(
+            collective_id=0, has_side_effects=True
+        ),
         name="decode_layer",
     )(
         tokens.T,
@@ -372,6 +405,18 @@
         up_weight,
         down_projection_weight,
     )
+    out, kp, nv = pl.pallas_call(
+        hand_over,
+        out_shape=(
+            jax.ShapeDtypeStruct((16, KV), BF16),
+            jax.ShapeDtypeStruct((KV, 128), BF16),
+            jax.ShapeDtypeStruct((KV, 128), BF16),
+        ),
+        in_specs=[vmem] * 3,
+        out_specs=(vmem, vmem, vmem),
+        compiler_params=pltpu.CompilerParams(vmem_limit_bytes=2**20),
+        name="hand_over",
+    )(out, kp, nv)
     return out.T, kp[:, None, :], nv[:, None, :]
 
 

time: 73.2 us -> 63.7 us (0.87)
  Pallas kernels: 68.4 us -> 62.9 us
  local copies, waits for them, and re-layouts: 3.86 us -> 0 us
    pallas_call x1 -> x2, Pallas kernels: 68.4 us -> 62.9 us  [the longest x1 62.3 us: shards(): pl.pallas_call(kernel, out_shape=(pltpu.VMEM((16, KV), BF16), pltpu.VMEM(...]
    unnamed x3 -> x0, local copies, waits for them, and re-layouts: 3.86 us -> none
where the time goes in v2:
time: 63.7 us; the launch traced here: 63.6 us
  Pallas kernels  62.9 us (99%)
  between operations  0.65 us (1%)
    pallas_call x1, Pallas kernels, shards(): pl.pallas_call(kernel, out_shape=(pltpu.VMEM((16, KV), BF16), pltpu.VMEM(...  62.3 us

profile of v2, /device:TPU:1, one launch (start us, length us, event | category | flops | bytes accessed | tf_op | source)
XLA Modules:
  0.0 63.6 jit_solution(4143007263545577594)
XLA Ops:
  0.6 62.3 %decode_layer.1 = (bf16[16,32]{1,0:T(8,128)(2,1)S(1)}, bf16[32,128]{1,0:T(8,128)(2,1)S(1)}, bf16[32,128]{1,0:T(8,128)(2,1)S(1)}) custom-call(bf16[16,32]{1,0:T(8,128)(2,1)} %bitcast.15, f32[1,128]{1,0:T(1,128)} %bitcast.16, bf16[128,256]{1,0:T(8,128)(2,1)} %wq1_h.1, bf16[128,256]{1,0:T(8,128)(2,1)} %wq2_h.1, bf16[64,128]{1,0:T(8,128)(2,1)} %bitcast.13, ...), custom_call_target="tpu_custom_call" | custom-call | tf_op jit(solution)/shard_map/decode_layer/pallas_call | solution.py:334
  63.0 0.6 hand_over.1
